TPU v7x, 32 devices: a whole 2x2x4 slice. The times are simulated.
32 devices in a mesh: sp: 8 (over z, x), tp: 4 (over y, core).
Axes of the slice: x: 2, y: 2, z: 4, core: 2. Of those that a mesh axis runs over, the one named last changes fastest.
Arguments:
- queries: bfloat16 [1024, 2048], P('sp', 'tp'), may hold values from -6 to 6
- keys: bfloat16 [1024, 512], P('sp', 'tp'), may hold values from -6 to 6
- values: bfloat16 [1024, 512], P('sp', 'tp'), may hold values from -6 to 6
- break_bias: float32 [16], P('tp'), as said below
- residual: bfloat16 [1024, 4096], P(('sp', 'tp')), may hold values from -6 to 6
- w_out: bfloat16 [2048, 4096], P('tp'), may hold values from -0.125 to 0.125
- ffn_gain: float32 [4096], replicated, may hold values from 0.1 to 1.9
- pick_ids: int32 [1024, 2], P('sp'), may hold values from 0 to 7, as said below
- pair_logit: float32 [1024], P('sp'), may hold values from -8 to 8
- w_gate: bfloat16 [8, 4096, 1024], P('sp', None, 'tp'), may hold values from -0.09375 to 0.09375
- w_up: bfloat16 [8, 4096, 1024], P('sp', None, 'tp'), may hold values from -0.09375 to 0.09375
- w_down: bfloat16 [8, 1024, 4096], P('sp', 'tp'), may hold values from -0.1875 to 0.1875
- out_gain: float32 [4096], replicated, may hold values from 0.1 to 1.9
Outputs:
- new_stream: bfloat16 [1024, 4096], P(('sp', 'tp'))
Inputs may be any that keep to these rules, and one draw needn't show every extreme that they name: `break_bias`: the logarithm of a break rate per position: between ln(0.02 / 1024) and ln(8 / 128). `pick_ids`: A row's 2 experts differ and lie in one group of 2 consecutive experts. In each aligned block of 32 rows no expert is named more than 12 times, and some expert exactly 12 times.
All inputs are finite; a program needn't handle non-finite values.
Results may differ from a plain program's by a relative error of at most 0.017.
Values may be sent and summed in bfloat16 or wider, within the bound.
A program may use at most 64 MiB of HBM per device.

v0:
```python
import jax
import jax.numpy as jnp
from jax import lax
from jax.sharding import PartitionSpec as P

HEAD = 128
TOP = 2
epsilon = 1e-06


def passed_along(block, axis, distance):
    devices = range(lax.axis_size(axis))
    route = [(i - distance, i) for i in devices if i - distance in devices]
    return lax.ppermute(block, axis, route)


def stick_block(carried, query_rows, key_block, value_block, head_bias, query_pos, key_pos, usable):
    output, used_up = carried
    scores = jnp.einsum("qcgd,scd->qcgs", query_rows, key_block, preferred_element_type=jnp.float32)
    scores = scores * query_rows.shape[-1] ** (-0.5) + head_bias[None, :, :, None]
    before = ((key_pos[None, :] < query_pos[:, None]) & usable)[:, None, None, :]
    breaks = jnp.where(before, jax.nn.softplus(scores), 0.0)
    behind = lax.cumsum(breaks, axis=3, reverse=True) - breaks
    weights = jnp.where(
        before, jnp.exp(jax.nn.log_sigmoid(scores) - behind - used_up[..., None]), 0.0
    )
    output = output + jnp.einsum(
        "qcgs,scd->qcgd",
        weights.astype(jnp.bfloat16),
        value_block,
        preferred_element_type=jnp.float32,
    )
    return (output, used_up + jnp.sum(breaks, axis=3))


def normed_heads(output):
    scaled = output * lax.rsqrt(jnp.mean(output * output, axis=-1, keepdims=True) + epsilon)
    return scaled.astype(jnp.bfloat16).reshape(output.shape[0], -1)


def on_device(
    queries,
    keys,
    values,
    break_bias,
    residual,
    w_out,
    ffn_gain,
    pick_ids,
    pair_logit,
    w_gate,
    w_up,
    w_down,
    out_gain,
):
    length = queries.shape[0]
    kv_local = keys.shape[1] // HEAD
    per_key = queries.shape[1] // keys.shape[1]
    query_rows = queries.reshape(length, kv_local, per_key, HEAD)
    head_bias = break_bias.reshape(kv_local, per_key)
    position = lax.axis_index("sp")
    offset = position * length
    query_pos = offset + jnp.arange(length, dtype=jnp.int32)
    initial = (
        jnp.zeros((length, kv_local, per_key, HEAD), jnp.float32),
        jnp.zeros((length, kv_local, per_key), jnp.float32),
    )
    stacked = jnp.stack([keys, values])
    carried = stick_block(
        initial,
        query_rows,
        keys.reshape(length, kv_local, HEAD),
        values.reshape(length, kv_local, HEAD),
        head_bias,
        query_pos,
        query_pos,
        True,
    )

    def visit(step_index, loop_state):
        arrived_pair, carried = loop_state
        arrived_pair = passed_along(arrived_pair, "sp", 1)
        source = position - step_index
        key_pos = source * length + jnp.arange(length, dtype=jnp.int32)
        carried = stick_block(
            carried,
            query_rows,
            arrived_pair[0].reshape(length, kv_local, HEAD),
            arrived_pair[1].reshape(length, kv_local, HEAD),
            head_bias,
            query_pos,
            key_pos,
            source >= 0,
        )
        return (arrived_pair, carried)

    head_out = normed_heads(lax.fori_loop(1, lax.axis_size("sp"), visit, (stacked, carried))[1][0])
    quarters = lax.axis_size("tp")
    quarter = lax.axis_index("tp")
    slice_rows = length // quarters
    width = w_out.shape[1]
    experts = lax.axis_size("sp")
    capacity = max(2, (3 * slice_rows + experts - 1) // experts)
    mixed = lax.psum_scatter(
        jnp.dot(head_out, w_out, preferred_element_type=jnp.float32).astype(jnp.bfloat16),
        "tp",
        scatter_dimension=0,
        tiled=True,
    ).astype(jnp.float32)
    stream = (residual.astype(jnp.float32) + mixed).astype(jnp.bfloat16)
    routed = lax.dynamic_slice_in_dim(pick_ids, quarter * slice_rows, slice_rows, 0)[None]
    stream_float = stream.astype(jnp.float32)
    ffn_in = (
        stream_float
        * lax.rsqrt(jnp.mean(stream_float * stream_float, axis=-1, keepdims=True) + epsilon)
        * ffn_gain
    ).astype(jnp.bfloat16)
    blocks = routed.shape[0]
    entries = ffn_in.reshape(blocks, slice_rows, width)
    flat_ids = routed.reshape(blocks, slice_rows * TOP)
    places = jnp.arange(slice_rows * TOP, dtype=jnp.int32)
    earlier = places[None, :] < places[:, None]
    matches = (flat_ids[:, :, None] == flat_ids[:, None, :]) & earlier[None]
    ranks = jnp.sum(matches.astype(jnp.int32), axis=2)
    targets = (flat_ids * capacity + ranks).reshape(blocks, slice_rows, TOP)
    block_ids = jnp.arange(blocks, dtype=jnp.int32)[:, None]
    outgoing = jnp.zeros((blocks, experts * capacity, width), jnp.bfloat16)
    for pick_index in range(TOP):
        outgoing = outgoing.at[block_ids, targets[:, :, pick_index]].set(entries)
    arrived = lax.all_to_all(outgoing, "sp", split_axis=1, concat_axis=1, tiled=True).reshape(
        -1, width
    )
    piece = lax.all_gather(arrived, "tp", axis=0, tiled=True)
    gated = jax.nn.silu(jnp.dot(piece, w_gate[0], preferred_element_type=jnp.float32))
    hidden = (gated * jnp.dot(piece, w_up[0], preferred_element_type=jnp.float32)).astype(
        jnp.bfloat16
    )
    results = lax.psum_scatter(
        jnp.dot(hidden, w_down[0], preferred_element_type=jnp.float32).astype(jnp.bfloat16),
        "tp",
        scatter_dimension=0,
        tiled=True,
    )
    returned = lax.all_to_all(results, "sp", split_axis=0, concat_axis=0, tiled=True)
    own_targets = targets[0]
    logits = lax.dynamic_slice_in_dim(pair_logit, quarter * slice_rows, slice_rows, 0)
    leading = returned[own_targets[:, 0]].astype(jnp.float32)
    trailing = returned[own_targets[:, 1]].astype(jnp.float32)
    blended = (
        jax.nn.sigmoid(logits)[:, None] * leading + jax.nn.sigmoid(-logits)[:, None] * trailing
    )
    blend_scale = lax.rsqrt(jnp.mean(blended * blended, axis=-1, keepdims=True) + epsilon)
    return (stream_float + blended * blend_scale * out_gain).astype(jnp.bfloat16)


def solution(mesh):
    placed = (
        P("sp", "tp"),
        P("sp", "tp"),
        P("sp", "tp"),
        P("tp"),
        P(("sp", "tp"), None),
        P("tp", None),
        P(),
        P("sp", None),
        P("sp"),
        P("sp", None, "tp"),
        P("sp", None, "tp"),
        P("sp", "tp", None),
        P(),
    )
    return jax.shard_map(
        on_device, mesh=mesh, in_specs=placed, out_specs=P(("sp", "tp"), None), check_vma=False
    )
```

profile of v0, /device:TPU:0, one launch (start us, length us, event | category | flops | bytes accessed | tf_op | source)
XLA Modules:
  0.0 276.8 jit_solution(1136986469250857039)
XLA Ops:
  6.7 1.1 copy.84
  8.0 1.3 fusion.82
  9.2 1.2 fusion.64
  11.0 62.2 %while.18 = (s32[]{:T(128)}, bf16[2,128,128]{2,1,0:T(8,128)(2,1)S(1)}, f32[128,1,4,128]{3,0,2,1:T(8,128)S(1)}, f32[128,1,4]{0,2,1:T(4,128)S(1)}, s32[]{:T(128)},...) while((s32[]{:T(128)}, ...), condition=%wide.region_5.6_spmd.clone, body=%wide.region_2.5_spmd.clone.sunk | while | flops 43942148 | bytes 2749119 | solution.py:97
  11.0 4.9 %collective-permute-start = (bf16[2,128,128]{2,1,0:T(8,128)(2,1)S(1)}, bf16[2,128,128]{2,1,0:T(8,128)(2,1)S(1)}, u32[]{:S(2)}, u32[]{:S(2)}) collective-permute-start(bf16[2,128,128]{2,1,0:T(8,128)(2,1)S(1)} %get-tuple-element.307), channel_id=1, source_target_pairs={{0,4},{4,8},{8,12},{12,16},{16,20},{20,24},{24,28},{1,5},{5,9},{9,... | collective-permute-start | bytes 196616 | tf_op jit(solution)/shard_map/while/body/eval_jaxpr/ppermute | solution.py:14
  16.0 1.8 collective-permute-done
  18.1 1.2 fusion.97
  19.9 4.3 %collective-permute-start = (bf16[2,128,128]{2,1,0:T(8,128)(2,1)S(1)}, bf16[2,128,128]{2,1,0:T(8,128)(2,1)S(1)}, u32[]{:S(2)}, u32[]{:S(2)}) collective-permute-start(bf16[2,128,128]{2,1,0:T(8,128)(2,1)S(1)} %get-tuple-element.307), channel_id=1, source_target_pairs={{0,4},{4,8},{8,12},{12,16},{16,20},{20,24},{24,28},{1,5},{5,9},{9,... | collective-permute-start | bytes 196616 | tf_op jit(solution)/shard_map/while/body/eval_jaxpr/ppermute | solution.py:14
  24.3 1.8 collective-permute-done
  26.4 1.2 fusion.97
  28.2 4.4 %collective-permute-start = (bf16[2,128,128]{2,1,0:T(8,128)(2,1)S(1)}, bf16[2,128,128]{2,1,0:T(8,128)(2,1)S(1)}, u32[]{:S(2)}, u32[]{:S(2)}) collective-permute-start(bf16[2,128,128]{2,1,0:T(8,128)(2,1)S(1)} %get-tuple-element.307), channel_id=1, source_target_pairs={{0,4},{4,8},{8,12},{12,16},{16,20},{20,24},{24,28},{1,5},{5,9},{9,... | collective-permute-start | bytes 196616 | tf_op jit(solution)/shard_map/while/body/eval_jaxpr/ppermute | solution.py:14
  32.6 1.8 collective-permute-done
  34.8 1.2 fusion.97
  36.5 5.2 %collective-permute-start = (bf16[2,128,128]{2,1,0:T(8,128)(2,1)S(1)}, bf16[2,128,128]{2,1,0:T(8,128)(2,1)S(1)}, u32[]{:S(2)}, u32[]{:S(2)}) collective-permute-start(bf16[2,128,128]{2,1,0:T(8,128)(2,1)S(1)} %get-tuple-element.307), channel_id=1, source_target_pairs={{0,4},{4,8},{8,12},{12,16},{16,20},{20,24},{24,28},{1,5},{5,9},{9,... | collective-permute-start | bytes 196616 | tf_op jit(solution)/shard_map/while/body/eval_jaxpr/ppermute | solution.py:14
  41.8 1.8 collective-permute-done
  44.0 1.2 fusion.97
  45.7 5.2 %collective-permute-start = (bf16[2,128,128]{2,1,0:T(8,128)(2,1)S(1)}, bf16[2,128,128]{2,1,0:T(8,128)(2,1)S(1)}, u32[]{:S(2)}, u32[]{:S(2)}) collective-permute-start(bf16[2,128,128]{2,1,0:T(8,128)(2,1)S(1)} %get-tuple-element.307), channel_id=1, source_target_pairs={{0,4},{4,8},{8,12},{12,16},{16,20},{20,24},{24,28},{1,5},{5,9},{9,... | collective-permute-start | bytes 196616 | tf_op jit(solution)/shard_map/while/body/eval_jaxpr/ppermute | solution.py:14
  51.0 1.8 collective-permute-done
  53.1 1.2 fusion.97
  54.9 5.2 %collective-permute-start = (bf16[2,128,128]{2,1,0:T(8,128)(2,1)S(1)}, bf16[2,128,128]{2,1,0:T(8,128)(2,1)S(1)}, u32[]{:S(2)}, u32[]{:S(2)}) collective-permute-start(bf16[2,128,128]{2,1,0:T(8,128)(2,1)S(1)} %get-tuple-element.307), channel_id=1, source_target_pairs={{0,4},{4,8},{8,12},{12,16},{16,20},{20,24},{24,28},{1,5},{5,9},{9,... | collective-permute-start | bytes 196616 | tf_op jit(solution)/shard_map/while/body/eval_jaxpr/ppermute | solution.py:14
  60.2 1.8 collective-permute-done
  62.3 1.2 fusion.97
  64.1 5.2 %collective-permute-start = (bf16[2,128,128]{2,1,0:T(8,128)(2,1)S(1)}, bf16[2,128,128]{2,1,0:T(8,128)(2,1)S(1)}, u32[]{:S(2)}, u32[]{:S(2)}) collective-permute-start(bf16[2,128,128]{2,1,0:T(8,128)(2,1)S(1)} %get-tuple-element.307), channel_id=1, source_target_pairs={{0,4},{4,8},{8,12},{12,16},{16,20},{20,24},{24,28},{1,5},{5,9},{9,... | collective-permute-start | bytes 196616 | tf_op jit(solution)/shard_map/while/body/eval_jaxpr/ppermute | solution.py:14
  69.4 1.8 collective-permute-done
  71.5 1.1 fusion.97
  73.6 4.0 %convolution_convert_fusion.1 = bf16[128,4096]{1,0:T(8,128)(2,1)} fusion(bf16[128,512]{0,1:T(8,128)(2,1)S(1)} %bitcast.134, bf16[512,4096]{1,0:T(8,128)(2,1)} %param.20), kind=kOutput, calls=%fused_computation.36 | convolution fusion | flops 537395200 | bytes 5373952 | tf_op jit(solution)/shard_map/dot_general | solution.py:105
  78.9 27.4 %reduce-scatter.3.cloned.1.call-done = bf16[32,4096]{1,0:T(8,128)(2,1)} async-done(((bf16[128,4096]{1,0:T(8,128)(2,1)}), bf16[32,4096]{1,0:T(8,128)(2,1)}) %reduce-scatter.3.cloned.1.call-update) | async-done | bytes 262160 | tf_op jit(solution)/shard_map/reduce_scatter | solution.py:104
  106.4 1.2 fusion.47
  107.6 1.3 scatter_custom_fusion
  108.9 1.7 scatter_custom_fusion.1
  110.6 2.9 %copy.126 = bf16[1,96,4096]{2,0,1:T(2,128)(2,1)} copy(bf16[1,96,4096]{2,1,0:T(8,128)(2,1)S(1)} %bitcast.132) | data formatting | bytes 1572864 | tf_op jit(solution)/shard_map/scatter | solution.py:129
  114.0 6.7 %reduce.14 = bf16[96,4096]{1,0:T(8,128)(2,1)S(1)} reduce(bf16[96,1,4096]{2,1,0:T(2,128)(2,1)} %bitcast.130, bf16[]{:T(256)} %broadcast.261), dimensions={1}, to_apply=%bitcast.113.reduce_sub_computation | reduce | bytes 1572866
  120.7 1.6 reshape.361
  122.3 25.5 %all_to_all.17 = bf16[8,2,24576]{2,1,0:T(2,128)(2,1)S(1)} all-to-all(bf16[8,2,24576]{2,1,0:T(2,128)(2,1)} %reshape.361), channel_id=1, replica_groups=mesh['sp'=8,'tp'=4] {'sp'}, dimensions={0} | all-to-all | bytes 1572864 | tf_op jit(solution)/shard_map/all_to_all | solution.py:130
  147.8 3.2 %reshape.362 = bf16[96,1,4096]{2,1,0:T(2,128)(2,1)} reshape(bf16[8,2,24576]{2,1,0:T(2,128)(2,1)S(1)} %all_to_all.17) | data formatting | bytes 1572864
  150.9 3.1 %copy.94 = bf16[1,96,4096]{2,1,0:T(8,128)(2,1)} copy(bf16[1,96,4096]{2,0,1:T(2,128)(2,1)} %bitcast.131) | data formatting | bytes 1572864 | tf_op jit(solution)/shard_map/all_to_all | solution.py:130
  154.2 26.7 %all-gather.3.cloned.1.call-done = bf16[1,384,4096]{2,1,0:T(8,128)(2,1)} async-done(((bf16[1,96,4096]{2,1,0:T(8,128)(2,1)}), bf16[1,384,4096]{2,1,0:T(8,128)(2,1)}) %all-gather.3.cloned.1.call-update) | async-done | bytes 3145744 | tf_op jit(solution)/shard_map/all_gather | solution.py:133
  180.9 3.5 %fusion.25 = f32[384,256]{1,0:T(8,128)S(1)} fusion(bf16[1,384,4096]{2,1,0:T(8,128)(2,1)} %all-gather.3.cloned.1.call-done, bf16[1,4096,256]{2,1,0:T(8,128)(2,1)} %param.24), kind=kOutput, calls=%fused_computation.39 | convolution fusion | flops 805306368 | bytes 5636096 | tf_op jit(solution)/shard_map/dot_general | solution.py:134
  184.4 7.7 %convolution_convert_fusion = bf16[384,4096]{1,0:T(8,128)(2,1)} fusion(bf16[1,256,4096]{2,1,0:T(8,128)(2,1)S(1)} %copy-done, bf16[1,4096,256]{2,1,0:T(8,128)(2,1)} %param.25, bf16[1,384,4096]{2,1,0:T(8,128)(2,1)} %all-gather.3.cloned.1.call-done, f32[384,256]{1,0:T(8,128)S(1)} %fusion.25), kind=kOutput, calls=%fused_computation.35 | convolution fusion | flops 1612775424 | bytes 10878976 | tf_op jit(solution)/shard_map/dot_general | solution.py:139
  192.1 38.0 %reduce-scatter.5.cloned.1.call-done = bf16[96,4096]{1,0:T(8,128)(2,1)} async-done(((bf16[384,4096]{1,0:T(8,128)(2,1)}), bf16[96,4096]{1,0:T(8,128)(2,1)}) %reduce-scatter.5.cloned.1.call-update) | async-done | bytes 786448 | tf_op jit(solution)/shard_map/reduce_scatter | solution.py:138
  230.2 2.2 all_to_all.12
  232.3 5.5 %all-to-all-start.1 = ((bf16[8,12,4096]{2,1,0:T(8,128)(2,1)}), bf16[8,12,4096]{2,1,0:T(8,128)(2,1)}, u32[]{:S(2)}, u32[]{:S(2)}) async-start(bf16[8,12,4096]{2,1,0:T(8,128)(2,1)} %all_to_all.12), calls=%async_computation.3 | async-start | bytes 2097152 | tf_op jit(solution)/shard_map/all_to_all | solution.py:144
  238.1 25.5 %all-to-all-done.1 = bf16[8,12,4096]{2,1,0:T(8,128)(2,1)} async-done(((bf16[8,12,4096]{2,1,0:T(8,128)(2,1)}), bf16[8,12,4096]{2,1,0:T(8,128)(2,1)}, u32[]{:S(2)}, u32[]{:S(2)}) %all-to-all-start.1) | async-done | bytes 786464 | tf_op jit(solution)/shard_map/all_to_all | solution.py:144
  263.6 1.4 all_to_all.14
  265.0 0.7 gather_fusion.1
  265.7 1.4 gather_fusion
  267.1 1.2 multiply_reduce_fusion
  268.4 1.9 fusion.50
  (98 shorter events, 10.5 us)
Async XLA Ops:
  6.5 177.9 %copy-start = (bf16[1,256,4096]{2,1,0:T(8,128)(2,1)S(1)}, bf16[1,256,4096]{2,1,0:T(8,128)(2,1)}, u32[]{:S(2)}) copy-start(bf16[1,256,4096]{2,1,0:T(8,128)(2,1)} %param.26) | copy-start | bytes 6291460
  6.5 4.5 %copy-start.8 = (f32[4]{0:T(128)S(1)}, f32[4]{0:T(128)}, u32[]{:S(2)}) copy-start(f32[4]{0:T(128)} %param.18) | copy-start | bytes 52
  6.5 3.9 %copy-start.3 = (bf16[128,128]{1,0:T(8,128)(2,1)S(1)}, bf16[128,128]{1,0:T(8,128)(2,1)}, u32[]{:S(2)}) copy-start(bf16[128,128]{1,0:T(8,128)(2,1)} %param.16) | copy-start | bytes 98308
  6.5 3.9 %copy-start.4 = (bf16[128,128]{1,0:T(8,128)(2,1)S(1)}, bf16[128,128]{1,0:T(8,128)(2,1)}, u32[]{:S(2)}) copy-start(bf16[128,128]{1,0:T(8,128)(2,1)} %param.17) | copy-start | bytes 98308
  6.5 99.8 %reduce-scatter.3.cloned.1.call-start = ((), (), s32[]{:S(2)}) async-start(), calls=%async_computation.4 | async-start | bytes 1310720 | tf_op jit(solution)/shard_map/reduce_scatter | solution.py:104
  11.0 6.8 %collective-permute-start = (bf16[2,128,128]{2,1,0:T(8,128)(2,1)S(1)}, bf16[2,128,128]{2,1,0:T(8,128)(2,1)S(1)}, u32[]{:S(2)}, u32[]{:S(2)}) collective-permute-start(bf16[2,128,128]{2,1,0:T(8,128)(2,1)S(1)} %get-tuple-element.307), channel_id=1, source_target_pairs={{0,4},{4,8},{8,12},{12,16},{16,20},{20,24},{24,28},{1,5},{5,9},{9,... | collective-permute-start | bytes 196616 | tf_op jit(solution)/shard_map/while/body/eval_jaxpr/ppermute | solution.py:14
  19.9 6.2 %collective-permute-start = (bf16[2,128,128]{2,1,0:T(8,128)(2,1)S(1)}, bf16[2,128,128]{2,1,0:T(8,128)(2,1)S(1)}, u32[]{:S(2)}, u32[]{:S(2)}) collective-permute-start(bf16[2,128,128]{2,1,0:T(8,128)(2,1)S(1)} %get-tuple-element.307), channel_id=1, source_target_pairs={{0,4},{4,8},{8,12},{12,16},{16,20},{20,24},{24,28},{1,5},{5,9},{9,... | collective-permute-start | bytes 196616 | tf_op jit(solution)/shard_map/while/body/eval_jaxpr/ppermute | solution.py:14
  28.2 6.2 %collective-permute-start = (bf16[2,128,128]{2,1,0:T(8,128)(2,1)S(1)}, bf16[2,128,128]{2,1,0:T(8,128)(2,1)S(1)}, u32[]{:S(2)}, u32[]{:S(2)}) collective-permute-start(bf16[2,128,128]{2,1,0:T(8,128)(2,1)S(1)} %get-tuple-element.307), channel_id=1, source_target_pairs={{0,4},{4,8},{8,12},{12,16},{16,20},{20,24},{24,28},{1,5},{5,9},{9,... | collective-permute-start | bytes 196616 | tf_op jit(solution)/shard_map/while/body/eval_jaxpr/ppermute | solution.py:14
  36.5 7.1 %collective-permute-start = (bf16[2,128,128]{2,1,0:T(8,128)(2,1)S(1)}, bf16[2,128,128]{2,1,0:T(8,128)(2,1)S(1)}, u32[]{:S(2)}, u32[]{:S(2)}) collective-permute-start(bf16[2,128,128]{2,1,0:T(8,128)(2,1)S(1)} %get-tuple-element.307), channel_id=1, source_target_pairs={{0,4},{4,8},{8,12},{12,16},{16,20},{20,24},{24,28},{1,5},{5,9},{9,... | collective-permute-start | bytes 196616 | tf_op jit(solution)/shard_map/while/body/eval_jaxpr/ppermute | solution.py:14
  45.7 7.1 %collective-permute-start = (bf16[2,128,128]{2,1,0:T(8,128)(2,1)S(1)}, bf16[2,128,128]{2,1,0:T(8,128)(2,1)S(1)}, u32[]{:S(2)}, u32[]{:S(2)}) collective-permute-start(bf16[2,128,128]{2,1,0:T(8,128)(2,1)S(1)} %get-tuple-element.307), channel_id=1, source_target_pairs={{0,4},{4,8},{8,12},{12,16},{16,20},{20,24},{24,28},{1,5},{5,9},{9,... | collective-permute-start | bytes 196616 | tf_op jit(solution)/shard_map/while/body/eval_jaxpr/ppermute | solution.py:14
  54.9 7.1 %collective-permute-start = (bf16[2,128,128]{2,1,0:T(8,128)(2,1)S(1)}, bf16[2,128,128]{2,1,0:T(8,128)(2,1)S(1)}, u32[]{:S(2)}, u32[]{:S(2)}) collective-permute-start(bf16[2,128,128]{2,1,0:T(8,128)(2,1)S(1)} %get-tuple-element.307), channel_id=1, source_target_pairs={{0,4},{4,8},{8,12},{12,16},{16,20},{20,24},{24,28},{1,5},{5,9},{9,... | collective-permute-start | bytes 196616 | tf_op jit(solution)/shard_map/while/body/eval_jaxpr/ppermute | solution.py:14
  64.1 7.1 %collective-permute-start = (bf16[2,128,128]{2,1,0:T(8,128)(2,1)S(1)}, bf16[2,128,128]{2,1,0:T(8,128)(2,1)S(1)}, u32[]{:S(2)}, u32[]{:S(2)}) collective-permute-start(bf16[2,128,128]{2,1,0:T(8,128)(2,1)S(1)} %get-tuple-element.307), channel_id=1, source_target_pairs={{0,4},{4,8},{8,12},{12,16},{16,20},{20,24},{24,28},{1,5},{5,9},{9,... | collective-permute-start | bytes 196616 | tf_op jit(solution)/shard_map/while/body/eval_jaxpr/ppermute | solution.py:14
  73.6 4.1 %copy-start.6 = (s32[128,2]{0,1:T(2,128)S(1)}, s32[128,2]{0,1:T(2,128)}, u32[]{:S(2)}) copy-start(s32[128,2]{0,1:T(2,128)} %param.22) | copy-start | bytes 3076
  73.6 32.8 %copy-start.1 = (bf16[32,4096]{1,0:T(8,128)(2,1)S(1)}, bf16[32,4096]{1,0:T(8,128)(2,1)}, u32[]{:S(2)}) copy-start(bf16[32,4096]{1,0:T(8,128)(2,1)} %param.19) | copy-start | bytes 786436
  77.6 30.0 %copy-start.2 = (f32[4096]{0:T(1024)S(1)}, f32[4096]{0:T(1024)}, u32[]{:S(2)}) copy-start(f32[4096]{0:T(1024)} %param.21) | copy-start | bytes 49156
  77.6 103.3 %all-gather.3.cloned.1.call-start = ((), (), s32[]{:S(2)}) async-start(), calls=%async_computation.6 | async-start | bytes 3932160 | tf_op jit(solution)/shard_map/all_gather | solution.py:133
  154.1 76.0 %reduce-scatter.5.cloned.1.call-start = ((), (), s32[]{:S(2)}) async-start(), calls=%async_computation.5 | async-start | bytes 3932160 | tf_op jit(solution)/shard_map/reduce_scatter | solution.py:138
  192.1 45.8 %copy-start.7 = (f32[128]{0:T(128)S(1)}, f32[128]{0:T(128)}, u32[]{:S(2)}) copy-start(f32[128]{0:T(128)} %param.23) | copy-start | bytes 1540
  232.3 31.3 %all-to-all-start.1 = ((bf16[8,12,4096]{2,1,0:T(8,128)(2,1)}), bf16[8,12,4096]{2,1,0:T(8,128)(2,1)}, u32[]{:S(2)}, u32[]{:S(2)}) async-start(bf16[8,12,4096]{2,1,0:T(8,128)(2,1)} %all_to_all.12), calls=%async_computation.3 | async-start | bytes 2097152 | tf_op jit(solution)/shard_map/all_to_all | solution.py:144
  265.0 3.4 %copy-start.5 = (f32[4096]{0:T(1024)S(1)}, f32[4096]{0:T(1024)}, u32[]{:S(2)}) copy-start(f32[4096]{0:T(1024)} %param.27) | copy-start | bytes 49156
Sparse Core Ops, SparseCore 0:
  77.7 28.6 reduce-scatter.2
  154.2 26.5 all-gather.2
  192.2 37.8 reduce-scatter.4
where the time goes:
time: 277 us
  waiting for transfers between devices  130 us (47%)
  starting transfers between devices  39.8 us (14%)
  blocking collectives  25.5 us (9%)
  other arithmetic  24.8 us (9%)
  matrix products  23.4 us (8%)
  local copies, waits for them, and re-layouts  19.4 us (7%)
  between operations  13.4 us (5%)
    reduce_scatter x1, waiting for transfers between devices, on_device(): lax.psum_scatter(jnp.dot(hidden, w_down[0], preferred_element_type=jnp.fl...  38 us
    ppermute x7, starting transfers between devices, passed_along(): return lax.ppermute(block, axis, route)  34.2 us
    reduce_scatter x1, waiting for transfers between devices, on_device(): lax.psum_scatter(jnp.dot(head_out, w_out, preferred_element_type=jnp.floa...  27.4 us
    all_gather x1, waiting for transfers between devices, on_device(): piece = lax.all_gather(arrived, 'tp', axis=0, tiled=True)  26.7 us
    all_to_all x1, waiting for transfers between devices, on_device(): lax.all_to_all(results, 'sp', split_axis=0, concat_axis=0, tiled=True)  25.5 us
    all_to_all x1, blocking collectives, on_device(): lax.all_to_all(outgoing, 'sp', split_axis=1, concat_axis=1, tiled=True)  25.5 us
    ppermute x7, waiting for transfers between devices, passed_along(): return lax.ppermute(block, axis, route)  12.4 us
    another operation x8, other arithmetic, stick_block(): behind = lax.cumsum(breaks, axis=3, reverse=True) - breaks  9.21 us
  transfers between devices with their start and end apart: 11, of which 11 were waited for; matrix products, arithmetic and copies ran while one was open for 1% of the time, Pallas kernels for 0%

commit v1 on v0

--- a/solution.py
+++ b/solution.py
@@ -127,9 +127,10 @@
     outgoing = jnp.zeros((blocks, experts * capacity, width), jnp.bfloat16)
     for pick_index in range(TOP):
         outgoing = outgoing.at[block_ids, targets[:, :, pick_index]].set(entries)
-    arrived = lax.all_to_all(outgoing, "sp", split_axis=1, concat_axis=1, tiled=True).reshape(
-        -1, width
-    )
+    arrived = jnp.concatenate(
+        lax.all_to_all(jnp.stack(jnp.split(outgoing, lax.axis_size("sp"), axis=1)), "sp", 0, 0),
+        axis=1,
+    ).reshape(-1, width)
     piece = lax.all_gather(arrived, "tp", axis=0, tiled=True)
     gated = jax.nn.silu(jnp.dot(piece, w_gate[0], preferred_element_type=jnp.float32))
     hidden = (gated * jnp.dot(piece, w_up[0], preferred_element_type=jnp.float32)).astype(

time: 277 us -> 267 us (0.964)
  local copies, waits for them, and re-layouts: 19.4 us -> 9.24 us
  other arithmetic: 24.8 us -> 18.7 us
  blocking collectives: 25.5 us -> 30.9 us
    unnamed x1 -> x0, other arithmetic: 6.65 us -> none
    all_to_all x1, blocking collectives: 25.5 us -> 30.9 us  [on_device(): lax.all_to_all(jnp.stack(jnp.split(outgoing, lax.axis_size('sp'), axis=1)...]
    unnamed x28, local copies, waits for them, and re-layouts: 7.1 us -> 1.93 us
    all_to_all x1 -> x0, local copies, waits for them, and re-layouts: 3.15 us -> none  [on_device(): lax.all_to_all(outgoing, 'sp', split_axis=1, concat_axis=1, tiled=True)]
    scatter x1 -> x0, local copies, waits for them, and re-layouts: 2.91 us -> none  [on_device(): outgoing = outgoing.at[block_ids, targets[:, :, pick_index]].set(entries)]
where the time goes in v1:
time: 267 us
  waiting for transfers between devices  130 us (49%)
  starting transfers between devices  39.9 us (15%)
  blocking collectives  30.9 us (12%)
  matrix products  24.1 us (9%)
  other arithmetic  18.7 us (7%)
  between operations  13.4 us (5%)
  local copies, waits for them, and re-layouts  9.24 us (3%)
    reduce_scatter x1, waiting for transfers between devices, on_device(): lax.psum_scatter(jnp.dot(hidden, w_down[0], preferred_element_type=jnp.fl...  38 us
    ppermute x7, starting transfers between devices, passed_along(): return lax.ppermute(block, axis, route)  34.2 us
    all_to_all x1, blocking collectives, on_device(): lax.all_to_all(jnp.stack(jnp.split(outgoing, lax.axis_size('sp'), axis=1)...  30.9 us
    reduce_scatter x1, waiting for transfers between devices, on_device(): lax.psum_scatter(jnp.dot(head_out, w_out, preferred_element_type=jnp.floa...  27.4 us
    all_gather x1, waiting for transfers between devices, on_device(): piece = lax.all_gather(arrived, 'tp', axis=0, tiled=True)  26.5 us
    all_to_all x1, waiting for transfers between devices, on_device(): lax.all_to_all(results, 'sp', split_axis=0, concat_axis=0, tiled=True)  25.5 us
    ppermute x7, waiting for transfers between devices, passed_along(): return lax.ppermute(block, axis, route)  12.4 us
    another operation x8, other arithmetic, stick_block(): behind = lax.cumsum(breaks, axis=3, reverse=True) - breaks  9.21 us
  transfers between devices with their start and end apart: 11, of which 11 were waited for; matrix products, arithmetic and copies ran while one was open for 1% of the time, Pallas kernels for 0%

profile of v1, /device:TPU:0, one launch (start us, length us, event | category | flops | bytes accessed | tf_op | source)
XLA Modules:
  0.0 266.7 jit_solution(14858983805950094947)
XLA Ops:
  6.6 1.2 copy.73
  7.9 1.3 fusion.82
  9.2 1.2 fusion.56
  10.4 0.8 pad_maximum_fusion
  11.1 1.3 convolution_bitcast_fusion.1
  12.5 62.2 %while.18 = (s32[]{:T(128)}, bf16[2,128,128]{2,1,0:T(8,128)(2,1)S(1)}, f32[128,1,4,128]{3,0,2,1:T(8,128)S(1)}, f32[128,1,4]{0,2,1:T(4,128)S(1)}, s32[]{:T(128)},...) while((s32[]{:T(128)}, ...), condition=%wide.region_5.6_spmd.clone, body=%wide.region_2.5_spmd.clone.sunk | while | flops 43942148 | bytes 2749119 | solution.py:97
  12.5 4.9 %collective-permute-start = (bf16[2,128,128]{2,1,0:T(8,128)(2,1)S(1)}, bf16[2,128,128]{2,1,0:T(8,128)(2,1)S(1)}, u32[]{:S(2)}, u32[]{:S(2)}) collective-permute-start(bf16[2,128,128]{2,1,0:T(8,128)(2,1)S(1)} %get-tuple-element.299), channel_id=1, source_target_pairs={{0,4},{4,8},{8,12},{12,16},{16,20},{20,24},{24,28},{1,5},{5,9},{9,... | collective-permute-start | bytes 196616 | tf_op jit(solution)/shard_map/while/body/eval_jaxpr/ppermute | solution.py:14
  17.5 1.8 collective-permute-done
  19.6 1.2 fusion.99
  21.3 4.3 %collective-permute-start = (bf16[2,128,128]{2,1,0:T(8,128)(2,1)S(1)}, bf16[2,128,128]{2,1,0:T(8,128)(2,1)S(1)}, u32[]{:S(2)}, u32[]{:S(2)}) collective-permute-start(bf16[2,128,128]{2,1,0:T(8,128)(2,1)S(1)} %get-tuple-element.299), channel_id=1, source_target_pairs={{0,4},{4,8},{8,12},{12,16},{16,20},{20,24},{24,28},{1,5},{5,9},{9,... | collective-permute-start | bytes 196616 | tf_op jit(solution)/shard_map/while/body/eval_jaxpr/ppermute | solution.py:14
  25.7 1.8 collective-permute-done
  27.9 1.2 fusion.99
  29.0 0.6 fusion.100
  29.6 4.4 %collective-permute-start = (bf16[2,128,128]{2,1,0:T(8,128)(2,1)S(1)}, bf16[2,128,128]{2,1,0:T(8,128)(2,1)S(1)}, u32[]{:S(2)}, u32[]{:S(2)}) collective-permute-start(bf16[2,128,128]{2,1,0:T(8,128)(2,1)S(1)} %get-tuple-element.299), channel_id=1, source_target_pairs={{0,4},{4,8},{8,12},{12,16},{16,20},{20,24},{24,28},{1,5},{5,9},{9,... | collective-permute-start | bytes 196616 | tf_op jit(solution)/shard_map/while/body/eval_jaxpr/ppermute | solution.py:14
  34.1 1.8 collective-permute-done
  36.2 1.2 fusion.99
  38.0 5.2 %collective-permute-start = (bf16[2,128,128]{2,1,0:T(8,128)(2,1)S(1)}, bf16[2,128,128]{2,1,0:T(8,128)(2,1)S(1)}, u32[]{:S(2)}, u32[]{:S(2)}) collective-permute-start(bf16[2,128,128]{2,1,0:T(8,128)(2,1)S(1)} %get-tuple-element.299), channel_id=1, source_target_pairs={{0,4},{4,8},{8,12},{12,16},{16,20},{20,24},{24,28},{1,5},{5,9},{9,... | collective-permute-start | bytes 196616 | tf_op jit(solution)/shard_map/while/body/eval_jaxpr/ppermute | solution.py:14
  43.3 1.8 collective-permute-done
  45.4 1.2 fusion.99
  46.6 0.6 fusion.100
  47.2 5.2 %collective-permute-start = (bf16[2,128,128]{2,1,0:T(8,128)(2,1)S(1)}, bf16[2,128,128]{2,1,0:T(8,128)(2,1)S(1)}, u32[]{:S(2)}, u32[]{:S(2)}) collective-permute-start(bf16[2,128,128]{2,1,0:T(8,128)(2,1)S(1)} %get-tuple-element.299), channel_id=1, source_target_pairs={{0,4},{4,8},{8,12},{12,16},{16,20},{20,24},{24,28},{1,5},{5,9},{9,... | collective-permute-start | bytes 196616 | tf_op jit(solution)/shard_map/while/body/eval_jaxpr/ppermute | solution.py:14
  52.5 1.8 collective-permute-done
  54.6 1.2 fusion.99
  56.4 5.2 %collective-permute-start = (bf16[2,128,128]{2,1,0:T(8,128)(2,1)S(1)}, bf16[2,128,128]{2,1,0:T(8,128)(2,1)S(1)}, u32[]{:S(2)}, u32[]{:S(2)}) collective-permute-start(bf16[2,128,128]{2,1,0:T(8,128)(2,1)S(1)} %get-tuple-element.299), channel_id=1, source_target_pairs={{0,4},{4,8},{8,12},{12,16},{16,20},{20,24},{24,28},{1,5},{5,9},{9,... | collective-permute-start | bytes 196616 | tf_op jit(solution)/shard_map/while/body/eval_jaxpr/ppermute | solution.py:14
  61.6 1.8 collective-permute-done
  63.8 1.2 fusion.99
  65.5 5.2 %collective-permute-start = (bf16[2,128,128]{2,1,0:T(8,128)(2,1)S(1)}, bf16[2,128,128]{2,1,0:T(8,128)(2,1)S(1)}, u32[]{:S(2)}, u32[]{:S(2)}) collective-permute-start(bf16[2,128,128]{2,1,0:T(8,128)(2,1)S(1)} %get-tuple-element.299), channel_id=1, source_target_pairs={{0,4},{4,8},{8,12},{12,16},{16,20},{20,24},{24,28},{1,5},{5,9},{9,... | collective-permute-start | bytes 196616 | tf_op jit(solution)/shard_map/while/body/eval_jaxpr/ppermute | solution.py:14
  70.8 1.8 collective-permute-done
  72.9 1.1 fusion.99
  75.1 4.0 %convolution_convert_fusion.1 = bf16[128,4096]{1,0:T(8,128)(2,1)} fusion(bf16[128,512]{0,1:T(8,128)(2,1)S(1)} %bitcast.158, bf16[512,4096]{1,0:T(8,128)(2,1)} %param.20), kind=kOutput, calls=%fused_computation.36 | convolution fusion | flops 537395200 | bytes 5373952 | tf_op jit(solution)/shard_map/dot_general | solution.py:105
  80.4 27.4 %reduce-scatter.3.cloned.1.call-done = bf16[32,4096]{1,0:T(8,128)(2,1)} async-done(((bf16[128,4096]{1,0:T(8,128)(2,1)}), bf16[32,4096]{1,0:T(8,128)(2,1)}) %reduce-scatter.3.cloned.1.call-update) | async-done | bytes 262160 | tf_op jit(solution)/shard_map/reduce_scatter | solution.py:104
  107.8 1.2 fusion.39
  109.0 1.3 scatter_custom_fusion
  110.3 1.5 scatter_custom_fusion.1
  112.1 30.9 %all_to_all.17 = bf16[8,1,12,4096]{3,2,1,0:T(8,128)(2,1)S(1)} all-to-all(bf16[8,1,12,4096]{3,2,1,0:T(8,128)(2,1)S(1)} %fusion.61), channel_id=1, replica_groups=mesh['sp'=8,'tp'=4] {'sp'}, dimensions={0} | all-to-all | bytes 1572864 | tf_op jit(solution)/shard_map/all_to_all | solution.py:131
  143.0 1.1 reshape_reshape.3
  144.3 26.5 %all-gather.2.cloned.1.call-done = bf16[384,4096]{1,0:T(8,128)(2,1)} async-done(((bf16[96,4096]{1,0:T(8,128)(2,1)}), bf16[384,4096]{1,0:T(8,128)(2,1)}) %all-gather.2.cloned.1.call-update) | async-done | bytes 3145744 | tf_op jit(solution)/shard_map/all_gather | solution.py:134
  170.8 3.5 %fusion.26 = f32[384,256]{1,0:T(8,128)S(1)} fusion(bf16[384,4096]{1,0:T(8,128)(2,1)} %all-gather.2.cloned.1.call-done, bf16[1,4096,256]{2,1,0:T(8,128)(2,1)} %param.24), kind=kOutput, calls=%fused_computation.40 | convolution fusion | flops 805306368 | bytes 5636096 | tf_op jit(solution)/shard_map/dot_general | solution.py:135
  174.3 7.7 %convolution_convert_fusion = bf16[384,4096]{1,0:T(8,128)(2,1)} fusion(bf16[1,256,4096]{2,1,0:T(8,128)(2,1)S(1)} %copy-done, bf16[384,4096]{1,0:T(8,128)(2,1)} %all-gather.2.cloned.1.call-done, bf16[1,4096,256]{2,1,0:T(8,128)(2,1)} %param.25, f32[384,256]{1,0:T(8,128)S(1)} %fusion.26), kind=kOutput, calls=%fused_computation.35 | convolution fusion | flops 1612775424 | bytes 10878976 | tf_op jit(solution)/shard_map/dot_general | solution.py:140
  182.0 38.0 %reduce-scatter.5.cloned.1.call-done = bf16[96,4096]{1,0:T(8,128)(2,1)} async-done(((bf16[384,4096]{1,0:T(8,128)(2,1)}), bf16[96,4096]{1,0:T(8,128)(2,1)}) %reduce-scatter.5.cloned.1.call-update) | async-done | bytes 786448 | tf_op jit(solution)/shard_map/reduce_scatter | solution.py:139
  220.1 2.2 all_to_all.12
  222.3 5.5 %all-to-all-start.1 = ((bf16[8,12,4096]{2,1,0:T(8,128)(2,1)}), bf16[8,12,4096]{2,1,0:T(8,128)(2,1)}, u32[]{:S(2)}, u32[]{:S(2)}) async-start(bf16[8,12,4096]{2,1,0:T(8,128)(2,1)} %all_to_all.12), calls=%async_computation.3 | async-start | bytes 2097152 | tf_op jit(solution)/shard_map/all_to_all | solution.py:145
  228.1 25.5 %all-to-all-done.1 = bf16[8,12,4096]{2,1,0:T(8,128)(2,1)} async-done(((bf16[8,12,4096]{2,1,0:T(8,128)(2,1)}), bf16[8,12,4096]{2,1,0:T(8,128)(2,1)}, u32[]{:S(2)}, u32[]{:S(2)}) %all-to-all-start.1) | async-done | bytes 786464 | tf_op jit(solution)/shard_map/all_to_all | solution.py:145
  253.6 1.4 all_to_all.14
  254.9 0.7 gather_fusion.1
  255.6 1.4 gather_fusion
  257.1 1.2 multiply_reduce_fusion
  258.3 1.9 fusion.42
  (97 shorter events, 8.6 us)
Async XLA Ops:
  6.5 167.8 %copy-start = (bf16[1,256,4096]{2,1,0:T(8,128)(2,1)S(1)}, bf16[1,256,4096]{2,1,0:T(8,128)(2,1)}, u32[]{:S(2)}) copy-start(bf16[1,256,4096]{2,1,0:T(8,128)(2,1)} %param.26) | copy-start | bytes 6291460
  6.5 5.9 %copy-start.6 = (f32[4]{0:T(128)S(1)}, f32[4]{0:T(128)}, u32[]{:S(2)}) copy-start(f32[4]{0:T(128)} %param.18) | copy-start | bytes 52
  6.5 101.3 %reduce-scatter.3.cloned.1.call-start = ((), (), s32[]{:S(2)}) async-start(), calls=%async_computation.4 | async-start | bytes 1310720 | tf_op jit(solution)/shard_map/reduce_scatter | solution.py:104
  12.5 6.8 %collective-permute-start = (bf16[2,128,128]{2,1,0:T(8,128)(2,1)S(1)}, bf16[2,128,128]{2,1,0:T(8,128)(2,1)S(1)}, u32[]{:S(2)}, u32[]{:S(2)}) collective-permute-start(bf16[2,128,128]{2,1,0:T(8,128)(2,1)S(1)} %get-tuple-element.299), channel_id=1, source_target_pairs={{0,4},{4,8},{8,12},{12,16},{16,20},{20,24},{24,28},{1,5},{5,9},{9,... | collective-permute-start | bytes 196616 | tf_op jit(solution)/shard_map/while/body/eval_jaxpr/ppermute | solution.py:14
  21.3 6.2 %collective-permute-start = (bf16[2,128,128]{2,1,0:T(8,128)(2,1)S(1)}, bf16[2,128,128]{2,1,0:T(8,128)(2,1)S(1)}, u32[]{:S(2)}, u32[]{:S(2)}) collective-permute-start(bf16[2,128,128]{2,1,0:T(8,128)(2,1)S(1)} %get-tuple-element.299), channel_id=1, source_target_pairs={{0,4},{4,8},{8,12},{12,16},{16,20},{20,24},{24,28},{1,5},{5,9},{9,... | collective-permute-start | bytes 196616 | tf_op jit(solution)/shard_map/while/body/eval_jaxpr/ppermute | solution.py:14
  29.6 6.2 %collective-permute-start = (bf16[2,128,128]{2,1,0:T(8,128)(2,1)S(1)}, bf16[2,128,128]{2,1,0:T(8,128)(2,1)S(1)}, u32[]{:S(2)}, u32[]{:S(2)}) collective-permute-start(bf16[2,128,128]{2,1,0:T(8,128)(2,1)S(1)} %get-tuple-element.299), channel_id=1, source_target_pairs={{0,4},{4,8},{8,12},{12,16},{16,20},{20,24},{24,28},{1,5},{5,9},{9,... | collective-permute-start | bytes 196616 | tf_op jit(solution)/shard_map/while/body/eval_jaxpr/ppermute | solution.py:14
  38.0 7.1 %collective-permute-start = (bf16[2,128,128]{2,1,0:T(8,128)(2,1)S(1)}, bf16[2,128,128]{2,1,0:T(8,128)(2,1)S(1)}, u32[]{:S(2)}, u32[]{:S(2)}) collective-permute-start(bf16[2,128,128]{2,1,0:T(8,128)(2,1)S(1)} %get-tuple-element.299), channel_id=1, source_target_pairs={{0,4},{4,8},{8,12},{12,16},{16,20},{20,24},{24,28},{1,5},{5,9},{9,... | collective-permute-start | bytes 196616 | tf_op jit(solution)/shard_map/while/body/eval_jaxpr/ppermute | solution.py:14
  47.2 7.1 %collective-permute-start = (bf16[2,128,128]{2,1,0:T(8,128)(2,1)S(1)}, bf16[2,128,128]{2,1,0:T(8,128)(2,1)S(1)}, u32[]{:S(2)}, u32[]{:S(2)}) collective-permute-start(bf16[2,128,128]{2,1,0:T(8,128)(2,1)S(1)} %get-tuple-element.299), channel_id=1, source_target_pairs={{0,4},{4,8},{8,12},{12,16},{16,20},{20,24},{24,28},{1,5},{5,9},{9,... | collective-permute-start | bytes 196616 | tf_op jit(solution)/shard_map/while/body/eval_jaxpr/ppermute | solution.py:14
  56.4 7.1 %collective-permute-start = (bf16[2,128,128]{2,1,0:T(8,128)(2,1)S(1)}, bf16[2,128,128]{2,1,0:T(8,128)(2,1)S(1)}, u32[]{:S(2)}, u32[]{:S(2)}) collective-permute-start(bf16[2,128,128]{2,1,0:T(8,128)(2,1)S(1)} %get-tuple-element.299), channel_id=1, source_target_pairs={{0,4},{4,8},{8,12},{12,16},{16,20},{20,24},{24,28},{1,5},{5,9},{9,... | collective-permute-start | bytes 196616 | tf_op jit(solution)/shard_map/while/body/eval_jaxpr/ppermute | solution.py:14
  65.5 7.1 %collective-permute-start = (bf16[2,128,128]{2,1,0:T(8,128)(2,1)S(1)}, bf16[2,128,128]{2,1,0:T(8,128)(2,1)S(1)}, u32[]{:S(2)}, u32[]{:S(2)}) collective-permute-start(bf16[2,128,128]{2,1,0:T(8,128)(2,1)S(1)} %get-tuple-element.299), channel_id=1, source_target_pairs={{0,4},{4,8},{8,12},{12,16},{16,20},{20,24},{24,28},{1,5},{5,9},{9,... | collective-permute-start | bytes 196616 | tf_op jit(solution)/shard_map/while/body/eval_jaxpr/ppermute | solution.py:14
  75.0 4.1 %copy-start.4 = (s32[128,2]{0,1:T(2,128)S(1)}, s32[128,2]{0,1:T(2,128)}, u32[]{:S(2)}) copy-start(s32[128,2]{0,1:T(2,128)} %param.22) | copy-start | bytes 3076
  75.1 32.8 %copy-start.1 = (bf16[32,4096]{1,0:T(8,128)(2,1)S(1)}, bf16[32,4096]{1,0:T(8,128)(2,1)}, u32[]{:S(2)}) copy-start(bf16[32,4096]{1,0:T(8,128)(2,1)} %param.19) | copy-start | bytes 786436
  75.1 33.9 %copy-start.2 = (f32[4096]{0:T(1024)S(1)}, f32[4096]{0:T(1024)}, u32[]{:S(2)}) copy-start(f32[4096]{0:T(1024)} %param.21) | copy-start | bytes 49156
  79.1 91.7 %all-gather.2.cloned.1.call-start = ((), (), s32[]{:S(2)}) async-start(), calls=%async_computation.5 | async-start | bytes 3932160 | tf_op jit(solution)/shard_map/all_gather | solution.py:134
  144.1 76.0 %reduce-scatter.5.cloned.1.call-start = ((), (), s32[]{:S(2)}) async-start(), calls=%async_computation.6 | async-start | bytes 3932160 | tf_op jit(solution)/shard_map/reduce_scatter | solution.py:139
  182.0 45.8 %copy-start.5 = (f32[128]{0:T(128)S(1)}, f32[128]{0:T(128)}, u32[]{:S(2)}) copy-start(f32[128]{0:T(128)} %param.23) | copy-start | bytes 1540
  222.3 31.3 %all-to-all-start.1 = ((bf16[8,12,4096]{2,1,0:T(8,128)(2,1)}), bf16[8,12,4096]{2,1,0:T(8,128)(2,1)}, u32[]{:S(2)}, u32[]{:S(2)}) async-start(bf16[8,12,4096]{2,1,0:T(8,128)(2,1)} %all_to_all.12), calls=%async_computation.3 | async-start | bytes 2097152 | tf_op jit(solution)/shard_map/all_to_all | solution.py:145
  228.1 30.2 %copy-start.3 = (f32[4096]{0:T(1024)S(1)}, f32[4096]{0:T(1024)}, u32[]{:S(2)}) copy-start(f32[4096]{0:T(1024)} %param.27) | copy-start | bytes 49156
Sparse Core Ops, SparseCore 0:
  79.2 28.5 reduce-scatter.2
  144.2 26.5 all-gather.1
  182.2 37.8 reduce-scatter.4
